TPU v7x, 32 devices: a whole 2x2x4 slice. The times are simulated.
32 devices in a mesh: rep: 2 (over y), fs: 4 (over z), tp: 4 (over x, core).
Axes of the slice: x: 2, y: 2, z: 4, core: 2. Of those that a mesh axis runs over, the one named last changes fastest.
Arguments:
- tokens: bfloat16 [2048, 2048], P(('rep', 'fs')), may hold values from -6 to 6
- gate_weight: bfloat16 [2048, 2816], P('fs', 'tp'), may hold values from -0.125 to 0.125
- up_weight: bfloat16 [2048, 2816], P('fs', 'tp'), may hold values from -0.125 to 0.125
- down_weight: bfloat16 [2816, 2048], P('tp', 'fs'), may hold values from -0.109375 to 0.109375
- out_grad: bfloat16 [2048, 2048], P(('rep', 'fs')), may hold values from -6 to 6
Outputs:
- input_grad: bfloat16 [2048, 2048], P(('rep', 'fs'))
- down_grad: float32 [2816, 2048], P('tp', 'fs')
- row_norms: float32 [2816], P('tp')
All inputs are finite; a program needn't handle non-finite values.
Results may differ from a plain program's by a relative error of at most 0.024.
Values may be sent and summed in bfloat16 or wider, within the bound.
A program may use at most 64 MiB of HBM per device.

v0:
```python
import jax
import jax.numpy as jnp
from jax import lax
from jax.sharding import PartitionSpec as P


def contract_last(left, right):
    return lax.dot_general(
        left, right, (((1,), (1,)), ((), ())), preferred_element_type=jnp.float32
    )


def contract_first(left, right):
    return lax.dot_general(
        left, right, (((0,), (0,)), ((), ())), preferred_element_type=jnp.float32
    )


def on_device(tokens, gate_weight, up_weight, down_weight, out_grad):
    down_full = lax.all_gather(down_weight, "fs", axis=1, tiled=True)
    gate_full, up_full = (
        lax.all_gather(gate_weight, "fs", axis=0, tiled=True),
        lax.all_gather(up_weight, "fs", axis=0, tiled=True),
    )
    gate_pre = jnp.dot(tokens, gate_full, preferred_element_type=jnp.float32)
    up_pre = jnp.dot(tokens, up_full, preferred_element_type=jnp.float32)
    sigma = jax.nn.sigmoid(gate_pre)
    activated = gate_pre * sigma
    hidden = (activated * up_pre).astype(jnp.bfloat16)
    hid_grad = contract_last(out_grad, down_full)
    up_grad = (hid_grad * activated).astype(jnp.bfloat16)
    gate_grad = (hid_grad * up_pre * sigma * (1.0 + gate_pre * (1.0 - sigma))).astype(jnp.bfloat16)
    partial_value = contract_last(gate_grad, gate_full) + contract_last(up_grad, up_full)
    input_grad = lax.psum(partial_value.astype(jnp.bfloat16), "tp")
    columns = lax.all_to_all(out_grad, "fs", split_axis=1, concat_axis=0, tiled=True)
    shard = contract_first(lax.all_gather(hidden, "fs", axis=0, tiled=True), columns)
    shard = lax.psum(shard.astype(jnp.bfloat16), "rep").astype(jnp.float32)
    norms = lax.psum(jnp.sum(shard * shard, axis=1), "fs")
    return (input_grad, shard, norms)


def solution(mesh):
    return jax.shard_map(
        on_device,
        mesh=mesh,
        in_specs=(
            P(("rep", "fs"), None),
            P("fs", "tp"),
            P("fs", "tp"),
            P("tp", "fs"),
            P(("rep", "fs"), None),
        ),
        out_specs=(P(("rep", "fs"), None), P("tp", "fs"), P("tp")),
        check_vma=False,
    )
```

profile of v0, /device:TPU:0, one launch (start us, length us, event | category | flops | bytes accessed | tf_op | source)
XLA Modules:
  0.0 329.1 jit_solution(854777100918134661)
XLA Ops:
  7.2 0.0 copy-start
  7.2 0.0 all-gather.9.cloned.1.call-start
  7.2 0.7 all-gather.9.cloned.1.call-update
  7.9 0.0 all-gather.7.cloned.1.call-start
  8.0 0.7 all-gather.7.cloned.1.call-update
  8.7 0.0 all-gather.5.cloned.1.call-start
  8.7 0.7 all-gather.5.cloned.1.call-update
  9.4 0.0 all-gather.11.cloned.1.call-start
  9.4 62.0 %all-gather.9.cloned.1.call-done = bf16[2048,704]{0,1:T(8,128)(2,1)} async-done(((bf16[512,704]{0,1:T(8,128)(2,1)}), bf16[2048,704]{0,1:T(8,128)(2,1)}) %all-gather.9.cloned.1.call-update) | async-done | bytes 2883600 | tf_op jit(solution)/shard_map/all_gather | solution.py:22
  71.4 0.0 copy-done
  71.4 2.8 fusion.8
  74.2 0.0 copy-start.3
  74.2 0.0 copy-start.2
  74.2 56.6 %all-gather.7.cloned.1.call-done = bf16[2048,704]{0,1:T(8,128)(2,1)} async-done(((bf16[512,704]{0,1:T(8,128)(2,1)}), bf16[2048,704]{0,1:T(8,128)(2,1)}) %all-gather.7.cloned.1.call-update) | async-done | bytes 2883600 | tf_op jit(solution)/shard_map/all_gather | solution.py:23
  130.8 3.7 %multiply_convert_fusion = (bf16[256,704]{0,1:T(8,128)(2,1)}, f32[256,704]{0,1:T(8,128)}) fusion(f32[256,704]{0,1:T(8,128)S(1)} %fusion.8, bf16[256,2048]{1,0:T(8,128)(2,1)S(1)} %copy-done, bf16[2048,704]{0,1:T(8,128)(2,1)} %all-gather.7.cloned.1.call-done), kind=kOutput, calls=%fused_computation.4 | convolution fusion | flops 739278848 | bytes 5734400 | tf_op jit(solution)/shard_map/dot_general | solution.py:26
  134.6 0.0 copy-done.3
  134.6 0.0 all-gather.11.cloned.1.call-update
  134.6 0.0 all-reduce.5.cloned.1.call-start
  134.6 0.0 copy-done.2
  134.7 0.5 copy.8
  135.2 56.6 %all_to_all.19 = bf16[256,4,512]{0,2,1:T(8,128)(2,1)S(1)} all-to-all(bf16[256,4,512]{0,2,1:T(8,128)(2,1)S(1)} %bitcast.14), channel_id=1, replica_groups=mesh['rep'=2,'fs'=4,'tp'=4] {'fs'}, dimensions={1} | all-to-all | bytes 2097152 | tf_op jit(solution)/shard_map/all_to_all | solution.py:35
  191.8 0.5 copy.9
  192.4 17.8 %all-gather.5.cloned.1.call-done = bf16[704,2048]{1,0:T(8,128)(2,1)} async-done(((bf16[704,512]{1,0:T(8,128)(2,1)}), bf16[704,2048]{1,0:T(8,128)(2,1)}) %all-gather.5.cloned.1.call-update) | async-done | bytes 2883600 | tf_op jit(solution)/shard_map/all_gather | solution.py:20
  210.1 3.9 %fusion.7 = f32[256,704]{0,1:T(8,128)} fusion(bf16[256,2048]{1,0:T(8,128)(2,1)} %param.9, bf16[704,2048]{1,0:T(8,128)(2,1)} %all-gather.5.cloned.1.call-done), kind=kOutput, calls=%fused_computation.13 | convolution fusion | flops 738197504 | bytes 4653056 | tf_op jit(solution)/shard_map/dot_general | solution.py:8
  214.1 32.2 %all-gather.11.cloned.1.call-done = bf16[1024,704]{0,1:T(8,128)(2,1)} async-done(((bf16[256,704]{0,1:T(8,128)(2,1)}), bf16[1024,704]{0,1:T(8,128)(2,1)}) %all-gather.11.cloned.1.call-update) | async-done | bytes 1441808 | tf_op jit(solution)/shard_map/all_gather | solution.py:36
  246.3 0.0 copy-start.4
  246.3 3.2 convolution_convert_fusion
  249.5 0.0 all-reduce.5.cloned.1.call-update
  249.5 0.0 all-reduce.3.cloned.1.call-start
  249.6 0.0 copy-done.4
  249.6 0.0 copy-start.1
  249.6 0.0 copy-start.5
  249.6 3.5 %fusion.2 = f32[256,2048]{1,0:T(8,128)S(1)} fusion(bf16[2048,704]{0,1:T(8,128)(2,1)} %all-gather.9.cloned.1.call-done, f32[256,704]{0,1:T(8,128)S(1)} %copy-done.4, f32[256,704]{0,1:T(8,128)} %fusion.7, f32[256,704]{0,1:T(8,128)} %get-tuple-element.6), kind=kOutput, calls=%fused_computation.9 | convolution fusion | flops 739999744 | bytes 7143424 | tf_op jit(solution)/shard_map/dot_general | solution.py:8
  253.1 0.0 copy-done.1
  253.1 0.0 copy-done.5
  253.1 2.0 fusion
  255.2 0.0 all-reduce.3.cloned.1.call-update
  255.2 25.6 %all-reduce.5.cloned.1.call-done = bf16[704,512]{1,0:T(8,128)(2,1)} async-done(((bf16[704,512]{1,0:T(8,128)(2,1)}), bf16[704,512]{1,0:T(8,128)(2,1)}) %all-reduce.5.cloned.1.call-update) | async-done | bytes 720912 | tf_op jit(solution)/shard_map/psum | solution.py:37
  280.8 2.3 multiply_reduce_fusion
  283.1 12.2 %psum.23 = f32[704]{0:T(1024)} all-reduce(f32[704]{0:T(1024)S(1)} %get-tuple-element.3), channel_id=1, replica_groups=mesh['rep'=2,'fs'=4,'tp'=4] {'fs'}, use_global_device_ids=true, to_apply=%region_3.0 | all-reduce | flops 704 | bytes 5632 | tf_op jit(solution)/shard_map/psum | solution.py:38
  295.4 24.5 %all-reduce.3.cloned.1.call-done = bf16[256,2048]{1,0:T(8,128)(2,1)} async-done(((bf16[256,2048]{1,0:T(8,128)(2,1)}), bf16[256,2048]{1,0:T(8,128)(2,1)}) %all-reduce.3.cloned.1.call-update) | async-done | bytes 1048592 | tf_op jit(solution)/shard_map/psum | solution.py:34
  319.9 2.3 copy.12
Async XLA Ops:
  7.2 64.3 %copy-start = (bf16[256,2048]{1,0:T(8,128)(2,1)S(1)}, bf16[256,2048]{1,0:T(8,128)(2,1)}, u32[]{:S(2)}) copy-start(bf16[256,2048]{1,0:T(8,128)(2,1)} %param.5) | copy-start | bytes 3145732
  7.2 64.2 %all-gather.9.cloned.1.call-start = ((), (), s32[]{:S(2)}) async-start(), calls=%async_computation.3 | async-start | bytes 3604480 | tf_op jit(solution)/shard_map/all_gather | solution.py:22
  7.9 122.9 %all-gather.7.cloned.1.call-start = ((), (), s32[]{:S(2)}) async-start(), calls=%async_computation.2 | async-start | bytes 3604480 | tf_op jit(solution)/shard_map/all_gather | solution.py:23
  8.7 201.5 %all-gather.5.cloned.1.call-start = ((), (), s32[]{:S(2)}) async-start(), calls=%async_computation.1 | async-start | bytes 3604480 | tf_op jit(solution)/shard_map/all_gather | solution.py:20
  9.4 236.9 %all-gather.11.cloned.1.call-start = ((), (), s32[]{:S(2)}) async-start(), calls=%async_computation.5 | async-start | bytes 1802240 | tf_op jit(solution)/shard_map/all_gather | solution.py:36
  74.2 60.4 %copy-start.3 = (f32[256,704]{0,1:T(8,128)}, f32[256,704]{0,1:T(8,128)S(1)}, u32[]{:S(2)}) copy-start(f32[256,704]{0,1:T(8,128)S(1)} %fusion.8) | copy-start | bytes 2162692
  74.2 60.4 %copy-start.2 = (bf16[256,2048]{1,0:T(8,128)(2,1)S(1)}, bf16[256,2048]{1,0:T(8,128)(2,1)}, u32[]{:S(2)}) copy-start(bf16[256,2048]{1,0:T(8,128)(2,1)} %param.9) | copy-start | bytes 3145732
  134.6 146.2 %all-reduce.5.cloned.1.call-start = ((), (), s32[]{:S(2)}) async-start(), calls=%async_computation.6 | async-start | bytes 1441792 | tf_op jit(solution)/shard_map/psum | solution.py:37
  246.3 3.3 %copy-start.4 = (f32[256,704]{0,1:T(8,128)S(1)}, f32[256,704]{0,1:T(8,128)}, u32[]{:S(2)}) copy-start(f32[256,704]{0,1:T(8,128)} %copy-done.3) | copy-start | bytes 2162692
  249.5 70.4 %all-reduce.3.cloned.1.call-start = ((), (), s32[]{:S(2)}) async-start(), calls=%async_computation.4 | async-start | bytes 2097152 | tf_op jit(solution)/shard_map/psum | solution.py:34
  249.6 3.5 %copy-start.1 = (bf16[2048,704]{0,1:T(8,128)(2,1)S(1)}, bf16[2048,704]{0,1:T(8,128)(2,1)}, u32[]{:S(2)}) copy-start(bf16[2048,704]{0,1:T(8,128)(2,1)} %all-gather.7.cloned.1.call-done) | copy-start | bytes 8650756
  249.6 3.5 %copy-start.5 = (f32[256,704]{0,1:T(8,128)S(1)}, f32[256,704]{0,1:T(8,128)}, u32[]{:S(2)}) copy-start(f32[256,704]{0,1:T(8,128)} %fusion.7) | copy-start | bytes 2162692
Sparse Core Ops, SparseCore 0:
  9.6 61.8 all-gather.8
  73.0 57.7 all-gather.6
  132.4 77.6 all-gather.4
  211.6 34.6 all-gather.10
  249.6 31.1 all-reduce.4
  283.6 36.2 all-reduce.2
where the time goes:
time: 329 us
  waiting for transfers between devices  221 us (67%)
  blocking collectives  68.9 us (21%)
  matrix products  19.2 us (6%)
  between operations  14.2 us (4%)
  local copies, waits for them, and re-layouts  3.4 us (1%)
    all_gather x1, waiting for transfers between devices, on_device(): lax.all_gather(gate_weight, 'fs', axis=0, tiled=True)  62 us
    all_to_all x1, blocking collectives, on_device(): lax.all_to_all(out_grad, 'fs', split_axis=1, concat_axis=0, tiled=True)  56.6 us
    all_gather x1, waiting for transfers between devices, on_device(): lax.all_gather(up_weight, 'fs', axis=0, tiled=True)  56.6 us
    all_gather x1, waiting for transfers between devices, on_device(): lax.all_gather(hidden, 'fs', axis=0, tiled=True)  32.2 us
    psum x1, waiting for transfers between devices, on_device(): shard = lax.psum(shard.astype(jnp.bfloat16), 'rep').astype(jnp.float32)  25.6 us
    psum x1, waiting for transfers between devices, on_device(): input_grad = lax.psum(partial_value.astype(jnp.bfloat16), 'tp')  24.5 us
    all_gather x1, waiting for transfers between devices, on_device(): down_full = lax.all_gather(down_weight, 'fs', axis=1, tiled=True)  17.8 us
    psum x1, blocking collectives, on_device(): norms = lax.psum(jnp.sum(shard * shard, axis=1), 'fs')  12.2 us
  transfers between devices with their start and end apart: 6, of which 6 were waited for; matrix products, arithmetic and copies ran while one was open for 6% of the time, Pallas kernels for 0%

commit v1 on v0

v1 whole, which is shorter than its diff:
```python
import functools

import jax
import jax.numpy as jnp
from jax import lax
from jax.experimental import pallas as pl
from jax.experimental.pallas import tpu as pltpu
from jax.sharding import PartitionSpec as P

MESH = pl.DeviceIdType.MESH
BF16 = jnp.bfloat16
F32 = jnp.float32


def contract_last(left, right):
    return lax.dot_general(left, right, (((1,), (1,)), ((), ())), preferred_element_type=F32)


def contract_first(left, right):
    return lax.dot_general(left, right, (((0,), (0,)), ((), ())), preferred_element_type=F32)


def gather_kernel(
    n, gate, up, down, tokens, grad, gate_all, up_all, down_all, tokens_all, grad_all,
    right_send, right_recv, left_send, left_recv, pair_send, pair_recv, own_sem,
):
    f = lax.axis_index("fs")
    r = lax.axis_index("rep")
    rows, width = tokens.shape[0], gate.shape[1]
    other = 1 - r

    barrier = pltpu.get_barrier_semaphore()
    for k in range(1, n):
        pl.semaphore_signal(barrier, inc=1, device_id={"fs": lax.rem(f + k, n)}, device_id_type=MESH)
    pl.semaphore_signal(barrier, inc=1, device_id={"rep": other}, device_id_type=MESH)
    pl.semaphore_wait(barrier, n)

    shards = ((gate, gate_all), (up, up_all), (down, down_all))

    def columns(owner):
        return pl.ds(pl.multiple_of(owner * width, width), width)

    def hop(w, step, right):
        own, whole = shards[w]
        owner = f - step if right else f + step
        place = whole.at[:, columns(owner)]
        return pltpu.make_async_remote_copy(
            src_ref=own if step == 0 else place,
            dst_ref=place,
            send_sem=(right_send if right else left_send).at[w, step],
            recv_sem=(right_recv if right else left_recv).at[w, step],
            device_id={"fs": f + 1 if right else f - 1},
            device_id_type=MESH,
        )

    def arrival(w, step, right):
        own, whole = shards[w]
        owner = f - 1 - step if right else f + 1 + step
        place = whole.at[:, columns(owner)]
        return pltpu.make_async_remote_copy(
            src_ref=place,
            dst_ref=place,
            send_sem=(right_send if right else left_send).at[w, step],
            recv_sem=(right_recv if right else left_recv).at[w, step],
            device_id={"fs": f - 1 if right else f + 1},
            device_id_type=MESH,
        )

    def sends(step, right):
        return (f < n - 1) & (f >= step) if right else (f > 0) & (f + step <= n - 1)

    def receives(step, right):
        return f - 1 - step >= 0 if right else f + 1 + step <= n - 1

    for w in range(3):
        for right in (True, False):
            @pl.when(sends(0, right))
            def _():
                hop(w, 0, right).start()

    pairs = []
    for i, (own, whole) in enumerate(((tokens, tokens_all), (grad, grad_all))):
        copy = pltpu.make_async_remote_copy(
            src_ref=own, dst_ref=whole.at[pl.ds(rows, rows)],
            send_sem=pair_send.at[i], recv_sem=pair_recv.at[i],
            device_id={"rep": other}, device_id_type=MESH,
        )
        copy.start()
        pairs.append(copy)
    local = []
    for i, (own, place) in enumerate((
        (tokens, tokens_all.at[pl.ds(0, rows)]),
        (grad, grad_all.at[pl.ds(0, rows)]),
        (gate, gate_all.at[:, columns(f)]),
        (up, up_all.at[:, columns(f)]),
        (down, down_all.at[:, columns(f)]),
    )):
        copy = pltpu.make_async_copy(own, place, own_sem.at[i])
        copy.start()
        local.append(copy)

    for step in range(n - 1):
        for w in range(3):
            for right in (True, False):
                @pl.when(receives(step, right))
                def _():
                    arrival(w, step, right).wait_recv()
                if step + 1 < n - 1:
                    @pl.when(sends(step + 1, right))
                    def _():
                        hop(w, step + 1, right).start()
    for step in range(n - 1):
        for w in range(3):
            for right in (True, False):
                @pl.when(sends(step, right))
                def _():
                    hop(w, step, right).wait_send()
    for copy in pairs:
        copy.wait()
    for copy in local:
        copy.wait()


def reduce_kernel(
    n, part, flow, input_grad, down_grad, norms,
    p_in, g_core, g_sum, g_rep, g_half, g_x, g_out, s_own, s_other, n_own, n_in,
    p_send, p_recv, g_send, g_recv, s_send, s_recv, n_send, n_recv,
):
    f = lax.axis_index("fs")
    r = lax.axis_index("rep")
    t = lax.axis_index("tp")
    c, x = lax.rem(t, 2), t // 2
    mate, far = x * 2 + 1 - c, (1 - x) * 2 + c
    units, width = p_in.shape[1], p_in.shape[2]
    rows = input_grad.shape[0]
    half, quarter = flow.shape[1] // 2, flow.shape[1] // 4

    barrier = pltpu.get_barrier_semaphore()
    peers = [{"rep": lax.rem(r + a, 2), "fs": lax.rem(f + k, n)}
             for a in range(2) for k in range(n) if a or k]
    for peer in peers + [{"tp": mate}, {"tp": far}]:
        pl.semaphore_signal(barrier, inc=1, device_id=peer, device_id_type=MESH)
    pl.semaphore_wait(barrier, 2 * n + 1)

    def cols(start, size):
        return pl.ds(pl.multiple_of(start, size), size)

    def push(i, src, dst, peer):
        copy = pltpu.make_async_remote_copy(
            src_ref=src, dst_ref=dst, send_sem=g_send.at[i], recv_sem=g_recv.at[i],
            device_id=peer, device_id_type=MESH,
        )
        copy.start()
        return copy

    first = push(0, flow.at[:, cols((1 - c) * half, half)], g_core, {"tp": mate})
    shards = []
    for k in range(1, n):
        to = lax.rem(f + k, n)
        copy = pltpu.make_async_remote_copy(
            src_ref=part.at[:, cols(to * width, width)], dst_ref=p_in.at[k - 1],
            send_sem=p_send.at[k - 1], recv_sem=p_recv.at[k - 1],
            device_id={"fs": to}, device_id_type=MESH,
        )
        copy.start()
        shards.append(copy)

    first.wait()
    for b in (1, 0):
        span = pl.ds(b * rows, rows)
        g_sum[b] = (flow[span, cols(c * half, half)].astype(F32) + g_core[span].astype(F32)).astype(BF16)
        if b == 1:
            second = push(1, g_sum.at[1], g_rep, {"rep": 1 - r})
    second.wait()
    for b in range(2):
        at = pl.ds(b * quarter, quarter)
        g_half[b] = (g_sum[0, :, at].astype(F32) + g_rep[:, at].astype(F32)).astype(BF16)
    third = push(2, g_half.at[1 - x], g_x, {"tp": far})
    third.wait()
    mine = cols(c * half + x * quarter, quarter)
    g_out[:, mine] = (g_half[x].astype(F32) + g_x[...].astype(F32)).astype(BF16)
    fourth = push(3, g_out.at[:, mine], g_out.at[:, mine], {"tp": far})

    total = part[:, cols(f * width, width)].astype(F32)
    for copy in shards:
        copy.wait()
    for k in range(n - 1):
        total = total + p_in[k].astype(F32)
    s_own[...] = total.astype(BF16)
    swap = pltpu.make_async_remote_copy(
        src_ref=s_own, dst_ref=s_other, send_sem=s_send, recv_sem=s_recv,
        device_id={"rep": 1 - r}, device_id_type=MESH,
    )
    swap.start()
    kept = s_own[...].astype(F32)
    down_grad[pl.ds(pl.multiple_of(r * units, 16), units), :] = kept
    n_own[...] = lax.dot_general(
        jnp.ones((8, width), F32), kept * kept, (((1,), (1,)), ((), ())),
        precision=lax.Precision.HIGHEST, preferred_element_type=F32,
    )
    small = []
    for i, peer in enumerate(peers):
        copy = pltpu.make_async_remote_copy(
            src_ref=n_own, dst_ref=n_in.at[i], send_sem=n_send.at[i], recv_sem=n_recv.at[i],
            device_id=peer, device_id_type=MESH,
        )
        copy.start()
        small.append(copy)

    fourth.wait()
    fifth = push(4, g_out.at[:, cols(c * half, half)], g_out.at[:, cols(c * half, half)], {"tp": mate})
    for copy in small:
        copy.wait()
    here = n_own[...]
    for i in range(n - 1):
        here = here + n_in[i]
    there = n_in[n - 1]
    for i in range(n, 2 * n - 1):
        there = there + n_in[i]
    norms[pl.ds(r, 1)] = here[None]
    norms[pl.ds(1 - r, 1)] = there[None]
    swap.wait()
    down_grad[pl.ds(pl.multiple_of((1 - r) * units, 16), units), :] = s_other[...].astype(F32)
    fifth.wait()
    input_grad[...] = g_out[...]


def split_units(n, tokens, gate_weight, up_weight, down_weight, out_grad):
    rows, depth = tokens.shape
    width, both = gate_weight.shape
    units = both // 2
    start = lax.axis_index("rep") * units
    gate = lax.dynamic_slice_in_dim(gate_weight, start, units, 1).T
    up = lax.dynamic_slice_in_dim(up_weight, start, units, 1).T
    down = lax.dynamic_slice_in_dim(down_weight, start, units, 0)
    vmem = pl.BlockSpec(memory_space=pltpu.VMEM)
    anywhere = pl.BlockSpec(memory_space=pl.ANY)
    dma = pltpu.SemaphoreType.DMA
    whole = jax.ShapeDtypeStruct((units, depth), BF16)
    stacked = jax.ShapeDtypeStruct((2 * rows, depth), BF16)
    gate, up, down, tokens, grad = pl.pallas_call(
        functools.partial(gather_kernel, n),
        out_shape=[whole, whole, whole, stacked, stacked],
        in_specs=[vmem] * 5,
        out_specs=[anywhere] * 5,
        scratch_shapes=[dma((3, n - 1))] * 4 + [dma((2,)), dma((2,)), dma((5,))],
        compiler_params=pltpu.CompilerParams(collective_id=0, has_side_effects=True),
        name="gather",
    )(gate, up, down, tokens, out_grad)

    gate_pre = contract_last(tokens, gate)
    up_pre = contract_last(tokens, up)
    sigma = jax.nn.sigmoid(gate_pre)
    activated = gate_pre * sigma
    hidden = (activated * up_pre).astype(BF16)
    hid_grad = contract_last(grad, down)
    up_grad = (hid_grad * activated).astype(BF16)
    gate_grad = (hid_grad * up_pre * sigma * (1.0 + gate_pre * (1.0 - sigma))).astype(BF16)
    part = contract_first(hidden, grad).astype(BF16)
    flow = (
        jnp.dot(gate_grad, gate, preferred_element_type=F32)
        + jnp.dot(up_grad, up, preferred_element_type=F32)
    ).astype(BF16)

    half, quarter = depth // 2, depth // 4
    peers = 2 * n - 1
    input_grad, down_grad, norms = pl.pallas_call(
        functools.partial(reduce_kernel, n),
        out_shape=[
            jax.ShapeDtypeStruct((rows, depth), BF16),
            jax.ShapeDtypeStruct((both, width), F32),
            jax.ShapeDtypeStruct((2, 8, units), F32),
        ],
        in_specs=[vmem] * 2,
        out_specs=[vmem] * 3,
        scratch_shapes=[
            pltpu.VMEM((n - 1, units, width), BF16),
            pltpu.VMEM((2 * rows, half), BF16),
            pltpu.VMEM((2, rows, half), BF16),
            pltpu.VMEM((rows, half), BF16),
            pltpu.VMEM((2, rows, quarter), BF16),
            pltpu.VMEM((rows, quarter), BF16),
            pltpu.VMEM((rows, depth), BF16),
            pltpu.VMEM((units, width), BF16),
            pltpu.VMEM((units, width), BF16),
            pltpu.VMEM((8, units), F32),
            pltpu.VMEM((peers, 8, units), F32),
            dma((n - 1,)), dma((n - 1,)), dma((5,)), dma((5,)), dma, dma, dma((peers,)), dma((peers,)),
        ],
        compiler_params=pltpu.CompilerParams(collective_id=1, has_side_effects=True),
        name="reduce",
    )(part, flow)
    return input_grad, down_grad, norms[:, 0, :].reshape(both)


def whole_units(tokens, gate_weight, up_weight, down_weight, out_grad):
    down_full = lax.all_gather(down_weight, "fs", axis=1, tiled=True)
    gate_full = lax.all_gather(gate_weight, "fs", axis=0, tiled=True)
    up_full = lax.all_gather(up_weight, "fs", axis=0, tiled=True)
    gate_pre = jnp.dot(tokens, gate_full, preferred_element_type=F32)
    up_pre = jnp.dot(tokens, up_full, preferred_element_type=F32)
    sigma = jax.nn.sigmoid(gate_pre)
    activated = gate_pre * sigma
    hidden = (activated * up_pre).astype(BF16)
    hid_grad = contract_last(out_grad, down_full)
    up_grad = (hid_grad * activated).astype(BF16)
    gate_grad = (hid_grad * up_pre * sigma * (1.0 + gate_pre * (1.0 - sigma))).astype(BF16)
    partial_value = contract_last(gate_grad, gate_full) + contract_last(up_grad, up_full)
    input_grad = lax.psum(partial_value.astype(BF16), "tp")
    columns = lax.all_to_all(out_grad, "fs", split_axis=1, concat_axis=0, tiled=True)
    shard = contract_first(lax.all_gather(hidden, "fs", axis=0, tiled=True), columns)
    shard = lax.psum(shard.astype(BF16), "rep").astype(F32)
    norms = lax.psum(jnp.sum(shard * shard, axis=1), "fs")
    return (input_grad, shard, norms)


def solution(mesh):
    n, rep, tp = mesh.shape["fs"], mesh.shape["rep"], mesh.shape["tp"]

    def on_device(tokens, gate_weight, up_weight, down_weight, out_grad):
        width, both = gate_weight.shape
        if rep == 2 and tp == 4 and 2 <= n <= 4 and both % 32 == 0 and width % 128 == 0:
            return split_units(n, tokens, gate_weight, up_weight, down_weight, out_grad)
        return whole_units(tokens, gate_weight, up_weight, down_weight, out_grad)

    return jax.shard_map(
        on_device,
        mesh=mesh,
        in_specs=(
            P(("rep", "fs"), None),
            P("fs", "tp"),
            P("fs", "tp"),
            P("tp", "fs"),
            P(("rep", "fs"), None),
        ),
        out_specs=(P(("rep", "fs"), None), P("tp", "fs"), P("tp")),
        check_vma=False,
    )
```

time: 329 us -> 145 us (0.44)
  waiting for transfers between devices: 221 us -> 0 us
  Pallas kernels: 0 us -> 122 us
  blocking collectives: 68.9 us -> 0 us
  between operations: 14.2 us -> 0.74 us
  matrix products: 19.2 us -> 11.4 us
  local copies, waits for them, and re-layouts: 3.4 us -> 9.8 us
    all_gather x4 -> x0, waiting for transfers between devices: 169 us -> none  [the longest x1 62 us: on_device(): lax.all_gather(gate_weight, 'fs', axis=0, tiled=True)]
    pallas_call x0 -> x2, Pallas kernels: none -> 122 us  [the longest x1 78 us: split_units(): pl.pallas_call(functools.partial(gather_kernel, n), out_shape=[whole, who...]
    all_to_all x1 -> x0, blocking collectives: 56.6 us -> none  [on_device(): lax.all_to_all(out_grad, 'fs', split_axis=1, concat_axis=0, tiled=True)]
    psum x2 -> x0, waiting for transfers between devices: 50.1 us -> none  [the longest x1 25.6 us: on_device(): shard = lax.psum(shard.astype(jnp.bfloat16), 'rep').astype(jnp.float32)]
    psum x1 -> x0, blocking collectives: 12.2 us -> none  [on_device(): norms = lax.psum(jnp.sum(shard * shard, axis=1), 'fs')]
    dot_general x3, matrix products: 9.5 us -> 5.05 us  [contract_last(): lax.dot_general(left, right, (((1,), (1,)), ((), ())), preferred_element_...]
  transfers between devices with their start and end apart: 6 -> 0, of which waited for: 6 -> 0; matrix products, arithmetic and copies ran while one was open for 6% -> 0% of each run, Pallas kernels for 0% -> 0%
where the time goes in v1:
time: 145 us; the launch traced here: 144 us
  Pallas kernels  122 us (84%)
  matrix products  11.4 us (8%)
  local copies, waits for them, and re-layouts  9.8 us (7%)
    pallas_call x1, Pallas kernels, split_units(): pl.pallas_call(functools.partial(gather_kernel, n), out_shape=[whole, who...  78 us
    pallas_call x1, Pallas kernels, split_units(): pl.pallas_call(functools.partial(reduce_kernel, n), out_shape=[jax.ShapeD...  43.8 us
    unnamed x14, local copies, waits for them, and re-layouts  5.49 us
    dot_general x3, matrix products, contract_last(): lax.dot_general(left, right, (((1,), (1,)), ((), ())), preferred_element_...  5.05 us

profile of v1, /device:TPU:0, one launch (start us, length us, event | category | flops | bytes accessed | tf_op | source)
XLA Modules:
  0.0 143.7 jit_solution(18069692043374166430)
XLA Ops:
  0.6 0.0 copy-start
  0.7 1.1 copy-done
  1.7 0.8 constant_dynamic-slice_fusion.down
  2.5 2.0 %dynamic-slice_bitcast_fusion = (bf16[352,512]{1,0:T(8,128)(2,1)}, bf16[352,512]{1,0:T(8,128)(2,1)}) fusion(bf16[512,704]{0,1:T(8,128)(2,1)} %param.7, s32[]{:T(128)S(6)} %select_n.2, bf16[512,704]{0,1:T(8,128)(2,1)} %param.6), kind=kLoop, calls=%fused_computation.9 | loop fusion | bytes 1441796 | tf_op jit(solution)/shard_map/transpose | solution.py:234
  4.5 78.0 %gather.1 = (bf16[352,2048]{1,0:T(8,128)(2,1)}, bf16[352,2048]{1,0:T(8,128)(2,1)}, bf16[352,2048]{1,0:T(8,128)(2,1)}, bf16[512,2048]{1,0:T(8,128)(2,1)}, bf16[512,2048]{1,0:T(8,128)(2,1)}) custom-call(bf16[352,512]{1,0:T(8,128)(2,1)} %get-tuple-element.20.gate, bf16[352,512]{1,0:T(8,128)(2,1)} %get-tuple-element.19.up, ...), custom_call_target="tpu_custom_call" | custom-call | tf_op jit(solution)/shard_map/gather/pallas_call | solution.py:241
  82.5 0.0 copy-start.3
  82.5 0.0 copy-start.5
  82.5 3.1 %fusion.10 = f32[512,352]{0,1:T(8,128)S(1)} fusion(bf16[512,2048]{1,0:T(8,128)(2,1)} %get-tuple-element.14, bf16[352,2048]{1,0:T(8,128)(2,1)} %get-tuple-element.15), kind=kOutput, calls=%fused_computation.18 | convolution fusion | flops 738197504 | bytes 4259840 | tf_op jit(solution)/shard_map/dot_general | solution.py:16
  85.6 0.0 copy-done.3
  85.6 0.0 copy-done.5
  85.6 0.0 copy-start.1
  85.6 0.9 fusion.8
  86.6 0.4 copy-done.1
  87.0 0.0 copy-start.4
  87.0 1.0 fusion.9
  88.0 0.6 copy-done.4
  88.6 2.1 %convolution_convert_fusion.part = bf16[352,2048]{1,0:T(8,128)(2,1)} fusion(bf16[512,2048]{1,0:T(8,128)(2,1)S(1)} %copy-done.4, f32[512,352]{0,1:T(8,128)S(1)} %fusion.9, f32[512,352]{0,1:T(8,128)S(1)} %fusion.8), kind=kOutput, calls=%fused_computation.1 | convolution fusion | flops 739999744 | bytes 4980736 | tf_op jit(solution)/shard_map/dot_general | solution.py:20
  90.7 1.5 %fusion.1 = f32[512,2048]{1,0:T(8,128)S(1)} fusion(bf16[352,2048]{1,0:T(8,128)(2,1)S(1)} %copy-done.3, f32[512,352]{0,1:T(8,128)S(1)} %fusion.8, f32[512,352]{0,1:T(8,128)S(1)} %fusion.10, f32[512,352]{0,1:T(8,128)S(1)} %fusion.9), kind=kOutput, calls=%fused_computation.7 | convolution fusion | flops 739999744 | bytes 7798784 | tf_op jit(solution)/shard_map/dot_general | solution.py:261
  92.1 2.8 %add_convert_fusion.flow = bf16[512,2048]{1,0:T(8,128)(2,1)} fusion(f32[512,2048]{1,0:T(8,128)S(1)} %fusion.1, bf16[352,2048]{1,0:T(8,128)(2,1)S(1)} %copy-done.1, f32[512,352]{0,1:T(8,128)S(1)} %fusion.10, f32[512,352]{0,1:T(8,128)S(1)} %fusion.8), kind=kOutput, calls=%fused_computation | convolution fusion | flops 741376000 | bytes 9175040 | tf_op jit(solution)/shard_map/dot_general | solution.py:262
  94.9 43.8 %reduce.3 = (bf16[256,2048]{1,0:T(8,128)(2,1)}, f32[704,512]{1,0:T(8,128)}, f32[2,8,352]{2,1,0:T(8,128)}) custom-call(bf16[352,2048]{1,0:T(8,128)(2,1)} %convolution_convert_fusion.part, bf16[512,2048]{1,0:T(8,128)(2,1)} %add_convert_fusion.flow), custom_call_target="tpu_custom_call" | custom-call | tf_op jit(solution)/shard_map/reduce/pallas_call | solution.py:267
  138.7 0.0 copy-start.2
  138.7 0.9 slice_reduce_fusion
  139.6 0.7 reshape_squeeze.3
  140.3 2.3 %copy.10 = bf16[256,2048]{1,0:T(8,128)(2,1)} copy(bf16[256,2048]{1,0:T(8,128)(2,1)} %get-tuple-element.24) | data formatting | bytes 2097152
  142.6 0.0 copy-done.2
  142.6 1.1 copy.11
Async XLA Ops:
  0.6 1.1 copy-start
  82.5 3.1 %copy-start.3 = (bf16[352,2048]{1,0:T(8,128)(2,1)S(1)}, bf16[352,2048]{1,0:T(8,128)(2,1)}, u32[]{:S(2)}) copy-start(bf16[352,2048]{1,0:T(8,128)(2,1)} %get-tuple-element.12) | copy-start | bytes 4325380
  82.5 3.1 %copy-start.5 = (bf16[512,2048]{1,0:T(8,128)(2,1)S(1)}, bf16[512,2048]{1,0:T(8,128)(2,1)}, u32[]{:S(2)}) copy-start(bf16[512,2048]{1,0:T(8,128)(2,1)} %get-tuple-element.11) | copy-start | bytes 6291460
  85.6 1.4 copy-start.1
  87.0 1.6 %copy-start.4 = (bf16[512,2048]{1,0:T(8,128)(2,1)S(1)}, bf16[512,2048]{1,0:T(8,128)(2,1)}, u32[]{:S(2)}) copy-start(bf16[512,2048]{1,0:T(8,128)(2,1)} %get-tuple-element.14) | copy-start | bytes 6291460
  138.7 3.9 %copy-start.2 = (f32[704,512]{1,0:T(8,128)S(1)}, f32[704,512]{1,0:T(8,128)}, u32[]{:S(2)}) copy-start(f32[704,512]{1,0:T(8,128)} %get-tuple-element.25) | copy-start | bytes 4325380

commit v2 on v0

v2 whole, which is shorter than its diff:
```python
import functools

import jax
import jax.numpy as jnp
from jax import lax
from jax.experimental import pallas as pl
from jax.experimental.pallas import tpu as pltpu
from jax.sharding import PartitionSpec as P

MESH = pl.DeviceIdType.MESH
BF16 = jnp.bfloat16
F32 = jnp.float32


def contract_last(left, right):
    return lax.dot_general(left, right, (((1,), (1,)), ((), ())), preferred_element_type=F32)


def contract_first(left, right):
    return lax.dot_general(left, right, (((0,), (0,)), ((), ())), preferred_element_type=F32)


def block_kernel(
    n, gate, up, down, tokens, grad, input_grad, down_grad, norms,
    gate_all, up_all, down_all, tokens_all, grad_all,
    gate_pre, up_pre, gate_grad, up_grad, part, p_in, p_out,
    f_out, f_in, g_own, g_out, g_in, h_out, h_in, whole_out, s_own, s_other, n_own, n_in,
    w_send, w_recv, p_send, p_recv, pair_send, pair_recv, own_sem, g_send, g_recv,
    s_send, s_recv, n_send, n_recv,
):
    f = lax.axis_index("fs")
    r = lax.axis_index("rep")
    t = lax.axis_index("tp")
    c, x = lax.rem(t, 2), t // 2
    mate, far = {"tp": x * 2 + 1 - c}, {"tp": (1 - x) * 2 + c}
    pair = {"rep": 1 - r}
    rows, depth = tokens.shape
    units, width = gate.shape
    half, quarter = depth // 2, depth // 4

    barrier = pltpu.get_barrier_semaphore()
    peers = [{"rep": lax.rem(r + a, 2), "fs": lax.rem(f + k, n)}
             for a in range(2) for k in range(n) if a or k]
    for peer in peers + [mate, far]:
        pl.semaphore_signal(barrier, inc=1, device_id=peer, device_id_type=MESH)
    pl.semaphore_wait(barrier, 2 * n + 1)

    def cols(start, size):
        return pl.ds(pl.multiple_of(start, size), size)

    def remote(src, dst, send, recv, peer):
        return pltpu.make_async_remote_copy(
            src_ref=src, dst_ref=dst, send_sem=send, recv_sem=recv,
            device_id=peer, device_id_type=MESH,
        )

    shards = ((gate, gate_all), (up, up_all), (down, down_all))
    ways = (1, 0)

    def hop(w, step, way, arriving=False):
        own, whole = shards[w]
        sign = 1 if way else -1
        owner = f - sign * (step + 1 if arriving else step)
        place = whole.at[:, cols(owner * width, width)]
        return remote(
            own if step == 0 and not arriving else place, place,
            w_send.at[way, w, step], w_recv.at[way, w, step],
            {"fs": f - sign if arriving else f + sign},
        )

    def sends(step, way):
        return (f < n - 1) & (f >= step) if way else (f > 0) & (f + step <= n - 1)

    def receives(step, way):
        return f - 1 - step >= 0 if way else f + 1 + step <= n - 1

    def forward(w, step):
        for way in ways:
            @pl.when(sends(step, way))
            def _():
                hop(w, step, way).start()

    def arrive(w, step):
        for way in ways:
            @pl.when(receives(step, way))
            def _():
                hop(w, step, way, True).wait_recv()

    for w in range(2):
        forward(w, 0)
    pairs = []
    for i, (own, whole) in enumerate(((tokens, tokens_all), (grad, grad_all))):
        copy = remote(own, whole.at[pl.ds(rows, rows)], pair_send.at[i], pair_recv.at[i], pair)
        copy.start()
        pairs.append(copy)
    local = []
    for i, (own, place) in enumerate((
        (tokens, tokens_all.at[pl.ds(0, rows)]),
        (grad, grad_all.at[pl.ds(0, rows)]),
        (gate, gate_all.at[:, cols(f * width, width)]),
        (up, up_all.at[:, cols(f * width, width)]),
        (down, down_all.at[:, cols(f * width, width)]),
    )):
        copy = pltpu.make_async_copy(own, place, own_sem.at[i])
        copy.start()
        local.append(copy)

    for step in range(n - 1):
        if step == n - 2:
            forward(2, 0)
        for w in range(2):
            arrive(w, step)
            if step + 1 < n - 1:
                forward(w, step + 1)
    for copy in pairs + local:
        copy.wait()

    for b in range(2):
        span = pl.ds(b * rows, rows)
        gate_pre[span] = contract_last(tokens_all[span], gate_all[...])
        up_pre[span] = contract_last(tokens_all[span], up_all[...])

    def relay_down(step):
        arrive(2, step)
        if step + 1 < n - 1:
            forward(2, step + 1)

    relay_down(0)
    pre = gate_pre[...]
    hidden = (pre * jax.nn.sigmoid(pre) * up_pre[...]).astype(BF16)
    for k in range(n):
        at = pl.ds(k * width, width)
        part[:, at] = contract_first(hidden, grad_all[:, at]).astype(BF16)

    def sum_goes(step, way):
        return f <= n - 2 - step if way else f >= step + 1

    def sum_comes(step, way):
        return (f >= 1) & (f <= n - 1 - step) if way else (f <= n - 2) & (f >= step)

    def sum_copy(step, way, first):
        target = n - 1 - step if way else step
        return remote(
            part.at[:, pl.ds(target * width, width)] if first else p_out.at[way, step],
            p_in.at[way, step], p_send.at[way, step], p_recv.at[way, step],
            {"fs": f + 1 if way else f - 1},
        )

    def at_end(way):
        return f == 0 if way else f == n - 1

    for step in range(n - 1):
        for way in ways:
            @pl.when(at_end(way))
            def _():
                sum_copy(step, way, True).start()

    def relay_sum(step):
        for way in ways:
            target = n - 1 - step if way else step

            @pl.when(sum_comes(step, way))
            def _():
                sum_copy(step, way, False).wait_recv()

            @pl.when(sum_comes(step, way) & sum_goes(step, way))
            def _():
                p_out[way, step] = (
                    part[:, pl.ds(target * width, width)].astype(F32) + p_in[way, step].astype(F32)
                ).astype(BF16)
                sum_copy(step, way, False).start()

    for step in range(1, n - 1):
        relay_down(step)

    for b in range(2):
        span = pl.ds(b * rows, rows)
        hid = contract_last(grad_all[span], down_all[...])
        pre = gate_pre[span]
        sigma = jax.nn.sigmoid(pre)
        up_grad[span] = (hid * (pre * sigma)).astype(BF16)
        gate_grad[span] = (hid * up_pre[span] * sigma * (1.0 + pre * (1.0 - sigma))).astype(BF16)

    def flow(b, at):
        span = pl.ds(b * rows, rows)
        return (
            jnp.dot(gate_grad[span], gate_all[:, at], preferred_element_type=F32)
            + jnp.dot(up_grad[span], up_all[:, at], preferred_element_type=F32)
        )

    def push(i, src, dst, peer):
        copy = remote(src, dst, g_send.at[i], g_recv.at[i], peer)
        copy.start()
        return copy

    cross = {}
    for b in (1, 0):
        f_out[b] = flow(b, cols((1 - c) * half, half)).astype(BF16)
        cross[b] = push(b, f_out.at[b], f_in.at[b], mate)
    for b in (1, 0):
        kept = flow(b, cols(c * half, half))
        cross[b].wait()
        kept = kept + f_in[b].astype(F32)
        for q in range(2):
            piece = kept[:, q * quarter:(q + 1) * quarter]
            if b == 1:
                g_out[q] = piece.astype(BF16)
            else:
                g_own[q] = piece
        if b == 1:
            early = push(2, g_out.at[1 - x], g_in.at[1 - x], pair)
            late = push(3, g_out.at[x], g_in.at[x], pair)
    relay_sum(0)
    early.wait()
    h_out[...] = (g_own[1 - x] + g_in[1 - x].astype(F32)).astype(BF16)
    over = push(4, h_out, h_in, far)
    for step in range(1, n - 1):
        relay_sum(step)

    def finish(way):
        step = n - 1 - f if way else f
        return p_in[way, lax.rem(step, n - 1)].astype(F32)

    s_sum = part[:, cols(f * width, width)].astype(F32)
    s_sum = s_sum + jnp.where(f > 0, finish(1), 0.0) + jnp.where(f < n - 1, finish(0), 0.0)
    s_own[...] = s_sum.astype(BF16)
    late.wait()
    over.wait()
    mine = cols(c * half + x * quarter, quarter)
    theirs = cols(c * half + (1 - x) * quarter, quarter)
    whole_out[:, mine] = (
        g_own[x] + g_in[x].astype(F32) + h_in[...].astype(F32)
    ).astype(BF16)
    across = push(5, whole_out.at[:, mine], whole_out.at[:, mine], far)
    beside = push(6, whole_out.at[:, mine], whole_out.at[:, mine], mate)
    swap = remote(s_own, s_other, s_send, s_recv, pair)
    swap.start()

    kept = s_own[...].astype(F32)
    down_grad[pl.ds(pl.multiple_of(r * units, 16), units), :] = kept
    n_own[...] = lax.dot_general(
        jnp.ones((8, width), F32), kept * kept, (((1,), (1,)), ((), ())),
        precision=lax.Precision.HIGHEST, preferred_element_type=F32,
    )
    small = []
    for i, peer in enumerate(peers):
        copy = remote(n_own, n_in.at[i], n_send.at[i], n_recv.at[i], peer)
        copy.start()
        small.append(copy)
    for step in range(n - 1):
        for way in ways:
            for w in range(3):
                @pl.when(sends(step, way))
                def _():
                    hop(w, step, way).wait_send()

            @pl.when(sum_goes(step, way))
            def _():
                sum_copy(step, way, False).wait_send()
    swap.wait()
    down_grad[pl.ds(pl.multiple_of((1 - r) * units, 16), units), :] = s_other[...].astype(F32)
    across.wait()
    last = push(7, whole_out.at[:, theirs], whole_out.at[:, theirs], mate)
    for copy in small:
        copy.wait()
    here = n_own[...]
    for i in range(n - 1):
        here = here + n_in[i]
    there = n_in[n - 1]
    for i in range(n, 2 * n - 1):
        there = there + n_in[i]
    norms[pl.ds(r, 1)] = here[None]
    norms[pl.ds(1 - r, 1)] = there[None]
    beside.wait()
    last.wait()
    input_grad[...] = whole_out[...]


def split_units(n, tokens, gate_weight, up_weight, down_weight, out_grad):
    rows, depth = tokens.shape
    width, both = gate_weight.shape
    units = both // 2
    start = lax.axis_index("rep") * units
    gate = lax.dynamic_slice_in_dim(gate_weight, start, units, 1).T
    up = lax.dynamic_slice_in_dim(up_weight, start, units, 1).T
    down = lax.dynamic_slice_in_dim(down_weight, start, units, 0)
    vmem = pl.BlockSpec(memory_space=pltpu.VMEM)
    dma = pltpu.SemaphoreType.DMA
    half, quarter = depth // 2, depth // 4
    peers = 2 * n - 1
    scratch = [((units, depth), BF16)] * 3 + [((2 * rows, depth), BF16)] * 2
    scratch += [((2 * rows, units), F32)] * 2 + [((2 * rows, units), BF16)] * 2
    scratch += [((units, depth), BF16)] + [((2, n - 1, units, width), BF16)] * 2
    scratch += [((2, rows, half), BF16)] * 2 + [((2, rows, quarter), F32)]
    scratch += [((2, rows, quarter), BF16)] * 2 + [((rows, quarter), BF16)] * 2
    scratch += [((rows, depth), BF16)] + [((units, width), BF16)] * 2
    scratch += [((8, units), F32), ((peers, 8, units), F32)]
    input_grad, down_grad, norms = pl.pallas_call(
        functools.partial(block_kernel, n),
        out_shape=[
            jax.ShapeDtypeStruct((rows, depth), BF16),
            jax.ShapeDtypeStruct((both, width), F32),
            jax.ShapeDtypeStruct((2, 8, units), F32),
        ],
        in_specs=[vmem] * 5,
        out_specs=[vmem] * 3,
        scratch_shapes=[pltpu.VMEM(shape, kind) for shape, kind in scratch] + [
            dma((2, 3, n - 1)), dma((2, 3, n - 1)), dma((2, n - 1)), dma((2, n - 1)),
            dma((2,)), dma((2,)), dma((5,)), dma((8,)), dma((8,)),
            dma, dma, dma((peers,)), dma((peers,)),
        ],
        compiler_params=pltpu.CompilerParams(collective_id=0, has_side_effects=True),
        name="block",
    )(gate, up, down, tokens, out_grad)
    return input_grad, down_grad, norms[:, 0, :].reshape(both)


def whole_units(tokens, gate_weight, up_weight, down_weight, out_grad):
    down_full = lax.all_gather(down_weight, "fs", axis=1, tiled=True)
    gate_full = lax.all_gather(gate_weight, "fs", axis=0, tiled=True)
    up_full = lax.all_gather(up_weight, "fs", axis=0, tiled=True)
    gate_pre = jnp.dot(tokens, gate_full, preferred_element_type=F32)
    up_pre = jnp.dot(tokens, up_full, preferred_element_type=F32)
    sigma = jax.nn.sigmoid(gate_pre)
    activated = gate_pre * sigma
    hidden = (activated * up_pre).astype(BF16)
    hid_grad = contract_last(out_grad, down_full)
    up_grad = (hid_grad * activated).astype(BF16)
    gate_grad = (hid_grad * up_pre * sigma * (1.0 + gate_pre * (1.0 - sigma))).astype(BF16)
    partial_value = contract_last(gate_grad, gate_full) + contract_last(up_grad, up_full)
    input_grad = lax.psum(partial_value.astype(BF16), "tp")
    columns = lax.all_to_all(out_grad, "fs", split_axis=1, concat_axis=0, tiled=True)
    shard = contract_first(lax.all_gather(hidden, "fs", axis=0, tiled=True), columns)
    shard = lax.psum(shard.astype(BF16), "rep").astype(F32)
    norms = lax.psum(jnp.sum(shard * shard, axis=1), "fs")
    return (input_grad, shard, norms)


def solution(mesh):
    n, rep, tp = mesh.shape["fs"], mesh.shape["rep"], mesh.shape["tp"]

    def on_device(tokens, gate_weight, up_weight, down_weight, out_grad):
        width, both = gate_weight.shape
        if rep == 2 and tp == 4 and 2 <= n <= 4 and both % 32 == 0 and width % 128 == 0:
            return split_units(n, tokens, gate_weight, up_weight, down_weight, out_grad)
        return whole_units(tokens, gate_weight, up_weight, down_weight, out_grad)

    return jax.shard_map(
        on_device,
        mesh=mesh,
        in_specs=(
            P(("rep", "fs"), None),
            P("fs", "tp"),
            P("fs", "tp"),
            P("tp", "fs"),
            P(("rep", "fs"), None),
        ),
        out_specs=(P(("rep", "fs"), None), P("tp", "fs"), P("tp")),
        check_vma=False,
    )
```

time: 329 us -> 123 us (0.37)
  waiting for transfers between devices: 221 us -> 0 us
  Pallas kernels: 0 us -> 114 us
  blocking collectives: 68.9 us -> 0 us
  matrix products: 19.2 us -> 0 us
  between operations: 14.2 us -> 0.66 us
  local copies, waits for them, and re-layouts: 3.4 us -> 8.8 us
    all_gather x4 -> x0, waiting for transfers between devices: 169 us -> none  [the longest x1 62 us: on_device(): lax.all_gather(gate_weight, 'fs', axis=0, tiled=True)]
    pallas_call x0 -> x1, Pallas kernels: none -> 114 us  [split_units(): pl.pallas_call(functools.partial(block_kernel, n), out_shape=[jax.ShapeDt...]
    all_to_all x1 -> x0, blocking collectives: 56.6 us -> none  [on_device(): lax.all_to_all(out_grad, 'fs', split_axis=1, concat_axis=0, tiled=True)]
    psum x2 -> x0, waiting for transfers between devices: 50.1 us -> none  [the longest x1 25.6 us: on_device(): shard = lax.psum(shard.astype(jnp.bfloat16), 'rep').astype(jnp.float32)]
    dot_general x6 -> x0, matrix products: 19.2 us -> none  [the longest x3 9.5 us: contract_last(): lax.dot_general(left, right, (((1,), (1,)), ((), ())), preferred_element_...]
    psum x1 -> x0, blocking collectives: 12.2 us -> none  [on_device(): norms = lax.psum(jnp.sum(shard * shard, axis=1), 'fs')]
  transfers between devices with their start and end apart: 6 -> 0, of which waited for: 6 -> 0; matrix products, arithmetic and copies ran while one was open for 6% -> 0% of each run, Pallas kernels for 0% -> 0%
where the time goes in v2:
time: 123 us
  Pallas kernels  114 us (93%)
  local copies, waits for them, and re-layouts  8.8 us (7%)
    pallas_call x1, Pallas kernels, split_units(): pl.pallas_call(functools.partial(block_kernel, n), out_shape=[jax.ShapeDt...  114 us
    unnamed x6, local copies, waits for them, and re-layouts  4.51 us

profile of v2, /device:TPU:0, one launch (start us, length us, event | category | flops | bytes accessed | tf_op | source)
XLA Modules:
  0.0 123.2 jit_solution(16744627691024466667)
XLA Ops:
  0.6 0.0 copy-start
  0.7 1.1 copy-done
  1.7 0.8 constant_dynamic-slice_fusion.down
  2.5 2.0 %dynamic-slice_bitcast_fusion = (bf16[352,512]{1,0:T(8,128)(2,1)}, bf16[352,512]{1,0:T(8,128)(2,1)}) fusion(bf16[512,704]{0,1:T(8,128)(2,1)} %param.7, s32[]{:T(128)S(6)} %select_n.2, bf16[512,704]{0,1:T(8,128)(2,1)} %param.6), kind=kLoop, calls=%fused_computation | loop fusion | bytes 1441796 | tf_op jit(solution)/shard_map/transpose | solution.py:285
  4.5 113.7 %block.1 = (bf16[256,2048]{1,0:T(8,128)(2,1)}, f32[704,512]{1,0:T(8,128)}, f32[2,8,352]{2,1,0:T(8,128)}) custom-call(bf16[352,512]{1,0:T(8,128)(2,1)} %get-tuple-element.10.gate, bf16[352,512]{1,0:T(8,128)(2,1)} %get-tuple-element.9.up, bf16[352,512]{1,0:T(8,128)(2,1)} %constant_dynamic-slice_fusion.down, bf16[256,2048]{1,0:T(8,128)(2,1)} %tokens.1, ...), custom_call_target="tpu_custom_call" | custom-call | tf_op jit(solution)/shard_map/block/pallas_call | solution.py:298
  118.2 0.0 copy-start.1
  118.3 0.9 slice_reduce_fusion
  119.1 0.7 reshape_squeeze.3
  119.8 2.3 %copy.10 = bf16[256,2048]{1,0:T(8,128)(2,1)} copy(bf16[256,2048]{1,0:T(8,128)(2,1)} %get-tuple-element.14) | data formatting | bytes 2097152
  122.1 0.0 copy-done.1
  122.1 1.1 copy.11
Async XLA Ops:
  0.6 1.1 copy-start
  118.2 3.9 %copy-start.1 = (f32[704,512]{1,0:T(8,128)S(1)}, f32[704,512]{1,0:T(8,128)}, u32[]{:S(2)}) copy-start(f32[704,512]{1,0:T(8,128)} %get-tuple-element.15) | copy-start | bytes 4325380

commit v3 on v2

--- a/solution.py
+++ b/solution.py
@@ -36,7 +36,10 @@
     pair = {"rep": 1 - r}
     rows, depth = tokens.shape
     units, width = gate.shape
-    half, quarter = depth // 2, depth // 4
+    half = depth // 2
+    pieces = g_out.shape[0]
+    size = half // pieces
+    down_half = down.at[pl.ds(pl.multiple_of(r * units, 16), units)]
 
     barrier = pltpu.get_barrier_semaphore()
     peers = [{"rep": lax.rem(r + a, 2), "fs": lax.rem(f + k, n)}
@@ -54,7 +57,7 @@
             device_id=peer, device_id_type=MESH,
         )
 
-    shards = ((gate, gate_all), (up, up_all), (down, down_all))
+    shards = ((gate, gate_all), (up, up_all), (down_half, down_all))
     ways = (1, 0)
 
     def hop(w, step, way, arriving=False):
@@ -99,7 +102,7 @@
         (grad, grad_all.at[pl.ds(0, rows)]),
         (gate, gate_all.at[:, cols(f * width, width)]),
         (up, up_all.at[:, cols(f * width, width)]),
-        (down, down_all.at[:, cols(f * width, width)]),
+        (down_half, down_all.at[:, cols(f * width, width)]),
     )):
         copy = pltpu.make_async_copy(own, place, own_sem.at[i])
         copy.start()
@@ -155,23 +158,34 @@
             def _():
                 sum_copy(step, way, True).start()
 
-    def relay_sum(step):
+    def relay_sum(step, hops):
         for way in ways:
             target = n - 1 - step if way else step
-
-            @pl.when(sum_comes(step, way))
+            here = f == hops if way else f == n - 1 - hops
+
+            @pl.when(sum_comes(step, way) & here)
             def _():
                 sum_copy(step, way, False).wait_recv()
 
-            @pl.when(sum_comes(step, way) & sum_goes(step, way))
+            @pl.when(sum_comes(step, way) & sum_goes(step, way) & here)
             def _():
                 p_out[way, step] = (
                     part[:, pl.ds(target * width, width)].astype(F32) + p_in[way, step].astype(F32)
                 ).astype(BF16)
                 sum_copy(step, way, False).start()
 
+    def relay_sums(when):
+        for step in range(n - 1):
+            hops = when - step
+            if 1 <= hops <= n - 1 - step:
+                relay_sum(step, hops)
+
     for step in range(1, n - 1):
         relay_down(step)
+        if step == 1:
+            relay_sums(1)
+    if n == 2:
+        relay_sums(1)
 
     for b in range(2):
         span = pl.ds(b * rows, rows)
@@ -197,25 +211,26 @@
     for b in (1, 0):
         f_out[b] = flow(b, cols((1 - c) * half, half)).astype(BF16)
         cross[b] = push(b, f_out.at[b], f_in.at[b], mate)
+    over = []
     for b in (1, 0):
         kept = flow(b, cols(c * half, half))
         cross[b].wait()
         kept = kept + f_in[b].astype(F32)
-        for q in range(2):
-            piece = kept[:, q * quarter:(q + 1) * quarter]
+        for q in range(pieces):
+            piece = kept[:, q * size:(q + 1) * size]
             if b == 1:
                 g_out[q] = piece.astype(BF16)
+                over.append(push(2 + q, g_out.at[q], g_in.at[q], pair))
             else:
                 g_own[q] = piece
-        if b == 1:
-            early = push(2, g_out.at[1 - x], g_in.at[1 - x], pair)
-            late = push(3, g_out.at[x], g_in.at[x], pair)
-    relay_sum(0)
-    early.wait()
-    h_out[...] = (g_own[1 - x] + g_in[1 - x].astype(F32)).astype(BF16)
-    over = push(4, h_out, h_in, far)
-    for step in range(1, n - 1):
-        relay_sum(step)
+    relay_sums(2)
+    across = []
+    for q in range(pieces):
+        over[q].wait()
+        h_out[q] = (g_own[q] + g_in[q].astype(F32)).astype(BF16)
+        across.append(push(2 + pieces + q, h_out.at[q], h_in.at[q], far))
+    for when in range(3, n):
+        relay_sums(when)
 
     def finish(way):
         step = n - 1 - f if way else f
@@ -224,20 +239,11 @@
     s_sum = part[:, cols(f * width, width)].astype(F32)
     s_sum = s_sum + jnp.where(f > 0, finish(1), 0.0) + jnp.where(f < n - 1, finish(0), 0.0)
     s_own[...] = s_sum.astype(BF16)
-    late.wait()
-    over.wait()
-    mine = cols(c * half + x * quarter, quarter)
-    theirs = cols(c * half + (1 - x) * quarter, quarter)
-    whole_out[:, mine] = (
-        g_own[x] + g_in[x].astype(F32) + h_in[...].astype(F32)
-    ).astype(BF16)
-    across = push(5, whole_out.at[:, mine], whole_out.at[:, mine], far)
-    beside = push(6, whole_out.at[:, mine], whole_out.at[:, mine], mate)
     swap = remote(s_own, s_other, s_send, s_recv, pair)
     swap.start()
 
     kept = s_own[...].astype(F32)
-    down_grad[pl.ds(pl.multiple_of(r * units, 16), units), :] = kept
+    down_grad[pl.ds(pl.multiple_of(r * units, 16), units), :] = s_own[...]
     n_own[...] = lax.dot_general(
         jnp.ones((8, width), F32), kept * kept, (((1,), (1,)), ((), ())),
         precision=lax.Precision.HIGHEST, preferred_element_type=F32,
@@ -247,6 +253,12 @@
         copy = remote(n_own, n_in.at[i], n_send.at[i], n_recv.at[i], peer)
         copy.start()
         small.append(copy)
+    beside = []
+    for q in range(pieces):
+        across[q].wait()
+        at = cols(c * half + q * size, size)
+        whole_out[:, at] = (h_out[q].astype(F32) + h_in[q].astype(F32)).astype(BF16)
+        beside.append(push(2 + 2 * pieces + q, whole_out.at[:, at], whole_out.at[:, at], mate))
     for step in range(n - 1):
         for way in ways:
             for w in range(3):
@@ -257,10 +269,6 @@
             @pl.when(sum_goes(step, way))
             def _():
                 sum_copy(step, way, False).wait_send()
-    swap.wait()
-    down_grad[pl.ds(pl.multiple_of((1 - r) * units, 16), units), :] = s_other[...].astype(F32)
-    across.wait()
-    last = push(7, whole_out.at[:, theirs], whole_out.at[:, theirs], mate)
     for copy in small:
         copy.wait()
     here = n_own[...]
@@ -269,10 +277,13 @@
     there = n_in[n - 1]
     for i in range(n, 2 * n - 1):
         there = there + n_in[i]
-    norms[pl.ds(r, 1)] = here[None]
-    norms[pl.ds(1 - r, 1)] = there[None]
-    beside.wait()
-    last.wait()
+    norms[...] = jnp.concatenate(
+        [jnp.where(r == 0, here, there), jnp.where(r == 0, there, here)], axis=1
+    )
+    swap.wait()
+    down_grad[pl.ds(pl.multiple_of((1 - r) * units, 16), units), :] = s_other[...]
+    for copy in beside:
+        copy.wait()
     input_grad[...] = whole_out[...]
 
 
@@ -283,36 +294,36 @@
     start = lax.axis_index("rep") * units
     gate = lax.dynamic_slice_in_dim(gate_weight, start, units, 1).T
     up = lax.dynamic_slice_in_dim(up_weight, start, units, 1).T
-    down = lax.dynamic_slice_in_dim(down_weight, start, units, 0)
+    anywhere = pl.BlockSpec(memory_space=pl.ANY)
     vmem = pl.BlockSpec(memory_space=pltpu.VMEM)
     dma = pltpu.SemaphoreType.DMA
-    half, quarter = depth // 2, depth // 4
+    half, pieces = depth // 2, 4
+    piece = (pieces, rows, half // pieces)
     peers = 2 * n - 1
     scratch = [((units, depth), BF16)] * 3 + [((2 * rows, depth), BF16)] * 2
     scratch += [((2 * rows, units), F32)] * 2 + [((2 * rows, units), BF16)] * 2
     scratch += [((units, depth), BF16)] + [((2, n - 1, units, width), BF16)] * 2
-    scratch += [((2, rows, half), BF16)] * 2 + [((2, rows, quarter), F32)]
-    scratch += [((2, rows, quarter), BF16)] * 2 + [((rows, quarter), BF16)] * 2
+    scratch += [((2, rows, half), BF16)] * 2 + [(piece, F32)] + [(piece, BF16)] * 4
     scratch += [((rows, depth), BF16)] + [((units, width), BF16)] * 2
     scratch += [((8, units), F32), ((peers, 8, units), F32)]
     input_grad, down_grad, norms = pl.pallas_call(
         functools.partial(block_kernel, n),
         out_shape=[
             jax.ShapeDtypeStruct((rows, depth), BF16),
-            jax.ShapeDtypeStruct((both, width), F32),
-            jax.ShapeDtypeStruct((2, 8, units), F32),
+            jax.ShapeDtypeStruct((both, width), BF16),
+            jax.ShapeDtypeStruct((8, both), F32),
         ],
-        in_specs=[vmem] * 5,
+        in_specs=[vmem] * 2 + [anywhere] * 3,
         out_specs=[vmem] * 3,
         scratch_shapes=[pltpu.VMEM(shape, kind) for shape, kind in scratch] + [
             dma((2, 3, n - 1)), dma((2, 3, n - 1)), dma((2, n - 1)), dma((2, n - 1)),
-            dma((2,)), dma((2,)), dma((5,)), dma((8,)), dma((8,)),
+            dma((2,)), dma((2,)), dma((5,)), dma((2 + 3 * pieces,)), dma((2 + 3 * pieces,)),
             dma, dma, dma((peers,)), dma((peers,)),
         ],
         compiler_params=pltpu.CompilerParams(collective_id=0, has_side_effects=True),
         name="block",
-    )(gate, up, down, tokens, out_grad)
-    return input_grad, down_grad, norms[:, 0, :].reshape(both)
+    )(gate, up, down_weight, tokens, out_grad)
+    return input_grad, down_grad.astype(F32), norms[0]
 
 
 def whole_units(tokens, gate_weight, up_weight, down_weight, out_grad):

time: 123 us -> 115 us (0.935)
  Pallas kernels: 114 us -> 107 us
  local copies, waits for them, and re-layouts: 8.8 us -> 4.4 us
  other arithmetic: 0 us -> 2.41 us
    pallas_call x1, Pallas kernels: 114 us -> 107 us  [split_units(): pl.pallas_call(functools.partial(block_kernel, n), out_shape=[jax.ShapeDt...]
    unnamed x6 -> x3, local copies, waits for them, and re-layouts: 4.51 us -> 0.97 us
    convert_element_type x0 -> x1, other arithmetic: none -> 2.41 us  [split_units(): return (input_grad, down_grad.astype(F32), norms[0])]
where the time goes in v3:
time: 115 us
  Pallas kernels  107 us (93%)
  local copies, waits for them, and re-layouts  4.4 us (4%)
  other arithmetic  2.41 us (2%)
    pallas_call x1, Pallas kernels, split_units(): pl.pallas_call(functools.partial(block_kernel, n), out_shape=[jax.ShapeDt...  107 us
    convert_element_type x1, other arithmetic, split_units(): return (input_grad, down_grad.astype(F32), norms[0])  2.41 us

profile of v3, /device:TPU:0, one launch (start us, length us, event | category | flops | bytes accessed | tf_op | source)
XLA Modules:
  0.0 114.7 jit_solution(10985212432513559735)
XLA Ops:
  0.6 2.0 %dynamic-slice_bitcast_fusion = (bf16[352,512]{1,0:T(8,128)(2,1)}, bf16[352,512]{1,0:T(8,128)(2,1)}) fusion(bf16[512,704]{0,1:T(8,128)(2,1)} %param.7, s32[]{:T(128)S(6)} %select_n.4, bf16[512,704]{0,1:T(8,128)(2,1)} %param.6), kind=kLoop, calls=%fused_computation | loop fusion | bytes 1441796 | tf_op jit(solution)/shard_map/transpose | solution.py:296
  2.6 107.2 %block.1 = (bf16[256,2048]{1,0:T(8,128)(2,1)}, bf16[704,512]{1,0:T(8,128)(2,1)}, f32[8,704]{1,0:T(8,128)}) custom-call(bf16[352,512]{1,0:T(8,128)(2,1)} %get-tuple-element.10.gate, bf16[352,512]{1,0:T(8,128)(2,1)} %get-tuple-element.9.up, bf16[704,512]{1,0:T(8,128)(2,1)} %down.1, bf16[256,2048]{1,0:T(8,128)(2,1)} %tokens.1, bf16[256,2048]{1,0:T(8,128)(2,1)} %grad.1), custom_call_target="tpu_custom_call" | custom-call | tf_op jit(solution)/shard_map/block/pallas_call | solution.py:309
  109.8 0.0 copy-start
  109.9 1.4 %slice_reduce_fusion = f32[704]{0:T(1024)} fusion(f32[8,704]{1,0:T(8,128)} %get-tuple-element.8), kind=kLoop, calls=%fused_computation.2 | loop fusion | bytes 5632 | tf_op jit(solution)/shard_map/slice | solution.py:326
  111.3 2.4 %convert_element_type.3 = f32[704,512]{1,0:T(8,128)} convert(bf16[704,512]{1,0:T(8,128)(2,1)} %get-tuple-element.7) | non-fusion elementwise | flops 360448 | bytes 2162688 | tf_op jit(solution)/shard_map/convert_element_type | solution.py:326
  113.7 0.0 copy-done
  113.7 1.0 copy.9
Async XLA Ops:
  109.8 3.8 %copy-start = (bf16[256,2048]{1,0:T(8,128)(2,1)S(1)}, bf16[256,2048]{1,0:T(8,128)(2,1)}, u32[]{:S(2)}) copy-start(bf16[256,2048]{1,0:T(8,128)(2,1)} %get-tuple-element.14) | copy-start | bytes 3145732

commit v4 on v3

--- a/solution.py
+++ b/solution.py
@@ -23,7 +23,7 @@
 def block_kernel(
     n, gate, up, down, tokens, grad, input_grad, down_grad, norms,
     gate_all, up_all, down_all, tokens_all, grad_all,
-    gate_pre, up_pre, gate_grad, up_grad, part, p_in, p_out,
+    gate_pre, up_pre, hid, gate_grad, up_grad, part, p_in, p_out,
     f_out, f_in, g_own, g_out, g_in, h_out, h_in, whole_out, s_own, s_other, n_own, n_in,
     w_send, w_recv, p_send, p_recv, pair_send, pair_recv, own_sem, g_send, g_recv,
     s_send, s_recv, n_send, n_recv,
@@ -129,8 +129,11 @@
             forward(2, step + 1)
 
     relay_down(0)
-    pre = gate_pre[...]
-    hidden = (pre * jax.nn.sigmoid(pre) * up_pre[...]).astype(BF16)
+    pre, raw = gate_pre[...], up_pre[...]
+    sigma = jax.nn.sigmoid(pre)
+    hidden = (pre * sigma * raw).astype(BF16)
+    gate_pre[...] = pre * sigma
+    up_pre[...] = raw * sigma * (1.0 + pre * (1.0 - sigma))
     for k in range(n):
         at = pl.ds(k * width, width)
         part[:, at] = contract_first(hidden, grad_all[:, at]).astype(BF16)
@@ -180,8 +183,22 @@
             if 1 <= hops <= n - 1 - step:
                 relay_sum(step, hops)
 
+    def add_shard(owner):
+        at = cols(owner * width, width)
+        hid[...] += contract_last(grad_all[:, at], down_all[:, at])
+
+    def add_shards(step):
+        for way in ways:
+            @pl.when(receives(step, way))
+            def _():
+                add_shard(f - 1 - step if way else f + 1 + step)
+
+    mine = cols(f * width, width)
+    hid[...] = contract_last(grad_all[:, mine], down_all[:, mine])
+    add_shards(0)
     for step in range(1, n - 1):
         relay_down(step)
+        add_shards(step)
         if step == 1:
             relay_sums(1)
     if n == 2:
@@ -189,11 +206,8 @@
 
     for b in range(2):
         span = pl.ds(b * rows, rows)
-        hid = contract_last(grad_all[span], down_all[...])
-        pre = gate_pre[span]
-        sigma = jax.nn.sigmoid(pre)
-        up_grad[span] = (hid * (pre * sigma)).astype(BF16)
-        gate_grad[span] = (hid * up_pre[span] * sigma * (1.0 + pre * (1.0 - sigma))).astype(BF16)
+        up_grad[span] = (hid[span] * gate_pre[span]).astype(BF16)
+        gate_grad[span] = (hid[span] * up_pre[span]).astype(BF16)
 
     def flow(b, at):
         span = pl.ds(b * rows, rows)
@@ -287,6 +301,12 @@
     input_grad[...] = whole_out[...]
 
 
+def write_kernel(flow, shard, rows, input_grad, down_grad, norms):
+    input_grad[...] = flow[...]
+    down_grad[...] = shard[...].astype(F32)
+    norms[...] = rows[0]
+
+
 def split_units(n, tokens, gate_weight, up_weight, down_weight, out_grad):
     rows, depth = tokens.shape
     width, both = gate_weight.shape
@@ -301,7 +321,7 @@
     piece = (pieces, rows, half // pieces)
     peers = 2 * n - 1
     scratch = [((units, depth), BF16)] * 3 + [((2 * rows, depth), BF16)] * 2
-    scratch += [((2 * rows, units), F32)] * 2 + [((2 * rows, units), BF16)] * 2
+    scratch += [((2 * rows, units), F32)] * 3 + [((2 * rows, units), BF16)] * 2
     scratch += [((units, depth), BF16)] + [((2, n - 1, units, width), BF16)] * 2
     scratch += [((2, rows, half), BF16)] * 2 + [(piece, F32)] + [(piece, BF16)] * 4
     scratch += [((rows, depth), BF16)] + [((units, width), BF16)] * 2
@@ -323,7 +343,17 @@
         compiler_params=pltpu.CompilerParams(collective_id=0, has_side_effects=True),
         name="block",
     )(gate, up, down_weight, tokens, out_grad)
-    return input_grad, down_grad.astype(F32), norms[0]
+    return tuple(pl.pallas_call(
+        write_kernel,
+        out_shape=[
+            jax.ShapeDtypeStruct((rows, depth), BF16),
+            jax.ShapeDtypeStruct((both, width), F32),
+            jax.ShapeDtypeStruct((both,), F32),
+        ],
+        in_specs=[vmem] * 3,
+        out_specs=[vmem] * 3,
+        name="write",
+    )(input_grad, down_grad, norms))
 
 
 def whole_units(tokens, gate_weight, up_weight, down_weight, out_grad):

time: 115 us -> 113 us (0.983)
  Pallas kernels: 107 us -> 110 us
  other arithmetic: 2.41 us -> 0 us
  local copies, waits for them, and re-layouts: 4.4 us -> 2 us
    pallas_call x0 -> x1, Pallas kernels: none -> 3.01 us  [split_units(): pl.pallas_call(write_kernel, out_shape=[jax.ShapeDtypeStruct((rows, depth...]
    convert_element_type x1 -> x0, other arithmetic: 2.41 us -> none  [split_units(): return (input_grad, down_grad.astype(F32), norms[0])]
    slice x1 -> x0, local copies, waits for them, and re-layouts: 1.43 us -> none  [split_units(): return (input_grad, down_grad.astype(F32), norms[0])]
where the time goes in v4:
time: 113 us; the launch traced here: 112 us
  Pallas kernels  110 us (97%)
  local copies, waits for them, and re-layouts  2 us (2%)
    pallas_call x1, Pallas kernels, split_units(): pl.pallas_call(functools.partial(block_kernel, n), out_shape=[jax.ShapeDt...  107 us
    pallas_call x1, Pallas kernels, split_units(): pl.pallas_call(write_kernel, out_shape=[jax.ShapeDtypeStruct((rows, depth...  3.01 us

profile of v4, /device:TPU:0, one launch (start us, length us, event | category | flops | bytes accessed | tf_op | source)
XLA Modules:
  0.0 112.3 jit_solution(13483487052910367106)
XLA Ops:
  0.6 2.0 %dynamic-slice_bitcast_fusion = (bf16[352,512]{1,0:T(8,128)(2,1)}, bf16[352,512]{1,0:T(8,128)(2,1)}) fusion(bf16[512,704]{0,1:T(8,128)(2,1)} %param.7, s32[]{:T(128)S(6)} %select_n.4, bf16[512,704]{0,1:T(8,128)(2,1)} %param.6), kind=kLoop, calls=%fused_computation | loop fusion | bytes 1441796 | tf_op jit(solution)/shard_map/transpose | solution.py:316
  2.6 106.7 %block.1 = (bf16[256,2048]{1,0:T(8,128)(2,1)}, bf16[704,512]{1,0:T(8,128)(2,1)}, f32[8,704]{1,0:T(8,128)}) custom-call(bf16[352,512]{1,0:T(8,128)(2,1)} %get-tuple-element.10.gate, bf16[352,512]{1,0:T(8,128)(2,1)} %get-tuple-element.9.up, bf16[704,512]{1,0:T(8,128)(2,1)} %down.1, bf16[256,2048]{1,0:T(8,128)(2,1)} %tokens.1, bf16[256,2048]{1,0:T(8,128)(2,1)} %grad.1), custom_call_target="tpu_custom_call" | custom-call | tf_op jit(solution)/shard_map/block/pallas_call | solution.py:329
  109.3 3.0 %write.1 = (bf16[256,2048]{1,0:T(8,128)(2,1)}, f32[704,512]{1,0:T(8,128)}, f32[704]{0:T(1024)}) custom-call(bf16[256,2048]{1,0:T(8,128)(2,1)} %get-tuple-element.6.flow, bf16[704,512]{1,0:T(8,128)(2,1)} %get-tuple-element.7.shard, f32[8,704]{1,0:T(8,128)} %get-tuple-element.8.rows), custom_call_target="tpu_custom_call" | custom-call | tf_op jit(solution)/shard_map/write/pallas_call | solution.py:346

commit v5 on v4

--- a/solution.py
+++ b/solution.py
@@ -36,7 +36,7 @@
     pair = {"rep": 1 - r}
     rows, depth = tokens.shape
     units, width = gate.shape
-    half = depth // 2
+    half, strip = depth // 2, width // 2
     pieces = g_out.shape[0]
     size = half // pieces
     down_half = down.at[pl.ds(pl.multiple_of(r * units, 16), units)]
@@ -144,11 +144,14 @@
     def sum_comes(step, way):
         return (f >= 1) & (f <= n - 1 - step) if way else (f <= n - 2) & (f >= step)
 
-    def sum_copy(step, way, first):
+    def lanes(k, base=0):
+        return pl.ds(base * width + k * strip, strip)
+
+    def sum_copy(step, way, k, first):
         target = n - 1 - step if way else step
         return remote(
-            part.at[:, pl.ds(target * width, width)] if first else p_out.at[way, step],
-            p_in.at[way, step], p_send.at[way, step], p_recv.at[way, step],
+            part.at[:, lanes(k, target)] if first else p_out.at[way, step, :, lanes(k)],
+            p_in.at[way, step, :, lanes(k)], p_send.at[way, step, k], p_recv.at[way, step, k],
             {"fs": f + 1 if way else f - 1},
         )
 
@@ -159,29 +162,30 @@
         for way in ways:
             @pl.when(at_end(way))
             def _():
-                sum_copy(step, way, True).start()
-
-    def relay_sum(step, hops):
+                for k in range(2):
+                    sum_copy(step, way, k, True).start()
+
+    def relay_sum(step, hops, k):
         for way in ways:
             target = n - 1 - step if way else step
             here = f == hops if way else f == n - 1 - hops
 
             @pl.when(sum_comes(step, way) & here)
             def _():
-                sum_copy(step, way, False).wait_recv()
+                sum_copy(step, way, k, False).wait_recv()
 
             @pl.when(sum_comes(step, way) & sum_goes(step, way) & here)
             def _():
-                p_out[way, step] = (
-                    part[:, pl.ds(target * width, width)].astype(F32) + p_in[way, step].astype(F32)
+                p_out[way, step, :, lanes(k)] = (
+                    part[:, lanes(k, target)].astype(F32) + p_in[way, step, :, lanes(k)].astype(F32)
                 ).astype(BF16)
-                sum_copy(step, way, False).start()
-
-    def relay_sums(when):
+                sum_copy(step, way, k, False).start()
+
+    def relay_sums(when, k):
         for step in range(n - 1):
             hops = when - step
             if 1 <= hops <= n - 1 - step:
-                relay_sum(step, hops)
+                relay_sum(step, hops, k)
 
     def add_shard(owner):
         at = cols(owner * width, width)
@@ -200,9 +204,11 @@
         relay_down(step)
         add_shards(step)
         if step == 1:
-            relay_sums(1)
+            relay_sums(1, 0)
+            relay_sums(1, 1)
     if n == 2:
-        relay_sums(1)
+        relay_sums(1, 0)
+        relay_sums(1, 1)
 
     for b in range(2):
         span = pl.ds(b * rows, rows)
@@ -227,6 +233,9 @@
         cross[b] = push(b, f_out.at[b], f_in.at[b], mate)
     over = []
     for b in (1, 0):
+        if b == 0:
+            for k in range(2):
+                relay_sums(2, k)
         kept = flow(b, cols(c * half, half))
         cross[b].wait()
         kept = kept + f_in[b].astype(F32)
@@ -237,25 +246,29 @@
                 over.append(push(2 + q, g_out.at[q], g_in.at[q], pair))
             else:
                 g_own[q] = piece
-    relay_sums(2)
     across = []
     for q in range(pieces):
         over[q].wait()
         h_out[q] = (g_own[q] + g_in[q].astype(F32)).astype(BF16)
         across.append(push(2 + pieces + q, h_out.at[q], h_in.at[q], far))
-    for when in range(3, n):
-        relay_sums(when)
-
-    def finish(way):
-        step = n - 1 - f if way else f
-        return p_in[way, lax.rem(step, n - 1)].astype(F32)
-
-    s_sum = part[:, cols(f * width, width)].astype(F32)
-    s_sum = s_sum + jnp.where(f > 0, finish(1), 0.0) + jnp.where(f < n - 1, finish(0), 0.0)
-    s_own[...] = s_sum.astype(BF16)
-    swap = remote(s_own, s_other, s_send, s_recv, pair)
-    swap.start()
-
+    swaps = []
+    for k in range(2):
+        for when in range(3, n):
+            relay_sums(when, k)
+
+        def finish(way):
+            step = n - 1 - f if way else f
+            return p_in[way, lax.rem(step, n - 1), :, lanes(k)].astype(F32)
+
+        at = pl.ds(pl.multiple_of(f * width + k * strip, strip), strip)
+        s_sum = part[:, at].astype(F32)
+        s_sum = s_sum + jnp.where(f > 0, finish(1), 0.0) + jnp.where(f < n - 1, finish(0), 0.0)
+        s_own[:, lanes(k)] = s_sum.astype(BF16)
+        copy = remote(
+            s_own.at[:, lanes(k)], s_other.at[:, lanes(k)], s_send.at[k], s_recv.at[k], pair
+        )
+        copy.start()
+        swaps.append(copy)
     kept = s_own[...].astype(F32)
     down_grad[pl.ds(pl.multiple_of(r * units, 16), units), :] = s_own[...]
     n_own[...] = lax.dot_general(
@@ -282,7 +295,8 @@
 
             @pl.when(sum_goes(step, way))
             def _():
-                sum_copy(step, way, False).wait_send()
+                for k in range(2):
+                    sum_copy(step, way, k, False).wait_send()
     for copy in small:
         copy.wait()
     here = n_own[...]
@@ -294,7 +308,8 @@
     norms[...] = jnp.concatenate(
         [jnp.where(r == 0, here, there), jnp.where(r == 0, there, here)], axis=1
     )
-    swap.wait()
+    for copy in swaps:
+        copy.wait()
     down_grad[pl.ds(pl.multiple_of((1 - r) * units, 16), units), :] = s_other[...]
     for copy in beside:
         copy.wait()
@@ -336,9 +351,9 @@
         in_specs=[vmem] * 2 + [anywhere] * 3,
         out_specs=[vmem] * 3,
         scratch_shapes=[pltpu.VMEM(shape, kind) for shape, kind in scratch] + [
-            dma((2, 3, n - 1)), dma((2, 3, n - 1)), dma((2, n - 1)), dma((2, n - 1)),
+            dma((2, 3, n - 1)), dma((2, 3, n - 1)), dma((2, n - 1, 2)), dma((2, n - 1, 2)),
             dma((2,)), dma((2,)), dma((5,)), dma((2 + 3 * pieces,)), dma((2 + 3 * pieces,)),
-            dma, dma, dma((peers,)), dma((peers,)),
+            dma((2,)), dma((2,)), dma((peers,)), dma((peers,)),
         ],
         compiler_params=pltpu.CompilerParams(collective_id=0, has_side_effects=True),
         name="block",
@@ -382,7 +397,7 @@
 
     def on_device(tokens, gate_weight, up_weight, down_weight, out_grad):
         width, both = gate_weight.shape
-        if rep == 2 and tp == 4 and 2 <= n <= 4 and both % 32 == 0 and width % 128 == 0:
+        if rep == 2 and tp == 4 and 2 <= n <= 4 and both % 32 == 0 and width % 256 == 0:
             return split_units(n, tokens, gate_weight, up_weight, down_weight, out_grad)
         return whole_units(tokens, gate_weight, up_weight, down_weight, out_grad)
 

time: 113 us -> 112 us (level)
  no operation moved by 1% of the time
where the time goes in v5:
time: 112 us
  Pallas kernels  110 us (98%)
  local copies, waits for them, and re-layouts  2 us (2%)
    pallas_call x1, Pallas kernels, split_units(): pl.pallas_call(functools.partial(block_kernel, n), out_shape=[jax.ShapeDt...  107 us
    pallas_call x1, Pallas kernels, split_units(): pl.pallas_call(write_kernel, out_shape=[jax.ShapeDtypeStruct((rows, depth...  3.01 us

profile of v5, /device:TPU:0, one launch (start us, length us, event | category | flops | bytes accessed | tf_op | source)
XLA Modules:
  0.0 112.2 jit_solution(3318918997488490144)
XLA Ops:
  0.6 2.0 %dynamic-slice_bitcast_fusion = (bf16[352,512]{1,0:T(8,128)(2,1)}, bf16[352,512]{1,0:T(8,128)(2,1)}) fusion(bf16[512,704]{0,1:T(8,128)(2,1)} %param.7, s32[]{:T(128)S(6)} %select_n.4, bf16[512,704]{0,1:T(8,128)(2,1)} %param.6), kind=kLoop, calls=%fused_computation | loop fusion | bytes 1441796 | tf_op jit(solution)/shard_map/transpose | solution.py:331
  2.6 106.5 %block.1 = (bf16[256,2048]{1,0:T(8,128)(2,1)}, bf16[704,512]{1,0:T(8,128)(2,1)}, f32[8,704]{1,0:T(8,128)}) custom-call(bf16[352,512]{1,0:T(8,128)(2,1)} %get-tuple-element.10.gate, bf16[352,512]{1,0:T(8,128)(2,1)} %get-tuple-element.9.up, bf16[704,512]{1,0:T(8,128)(2,1)} %down.1, bf16[256,2048]{1,0:T(8,128)(2,1)} %tokens.1, bf16[256,2048]{1,0:T(8,128)(2,1)} %grad.1), custom_call_target="tpu_custom_call" | custom-call | tf_op jit(solution)/shard_map/block/pallas_call | solution.py:344
  109.2 3.0 %write.1 = (bf16[256,2048]{1,0:T(8,128)(2,1)}, f32[704,512]{1,0:T(8,128)}, f32[704]{0:T(1024)}) custom-call(bf16[256,2048]{1,0:T(8,128)(2,1)} %get-tuple-element.6.flow, bf16[704,512]{1,0:T(8,128)(2,1)} %get-tuple-element.7.shard, f32[8,704]{1,0:T(8,128)} %get-tuple-element.8.rows), custom_call_target="tpu_custom_call" | custom-call | tf_op jit(solution)/shard_map/write/pallas_call | solution.py:361

commit v6 on v5

--- a/solution.py
+++ b/solution.py
@@ -332,7 +332,7 @@
     anywhere = pl.BlockSpec(memory_space=pl.ANY)
     vmem = pl.BlockSpec(memory_space=pltpu.VMEM)
     dma = pltpu.SemaphoreType.DMA
-    half, pieces = depth // 2, 4
+    half, pieces = depth // 2, 8
     piece = (pieces, rows, half // pieces)
     peers = 2 * n - 1
     scratch = [((units, depth), BF16)] * 3 + [((2 * rows, depth), BF16)] * 2

time: 112 us -> 113 us (level)
  no operation moved by 1% of the time
where the time goes in v6:
time: 113 us; the launch traced here: 112 us
  Pallas kernels  110 us (97%)
  local copies, waits for them, and re-layouts  2 us (2%)
    pallas_call x1, Pallas kernels, split_units(): pl.pallas_call(functools.partial(block_kernel, n), out_shape=[jax.ShapeDt...  107 us
    pallas_call x1, Pallas kernels, split_units(): pl.pallas_call(write_kernel, out_shape=[jax.ShapeDtypeStruct((rows, depth...  3.01 us

profile of v6, /device:TPU:0, one launch (start us, length us, event | category | flops | bytes accessed | tf_op | source)
XLA Modules:
  0.0 112.4 jit_solution(17978873019319501634)
XLA Ops:
  0.6 2.0 %dynamic-slice_bitcast_fusion = (bf16[352,512]{1,0:T(8,128)(2,1)}, bf16[352,512]{1,0:T(8,128)(2,1)}) fusion(bf16[512,704]{0,1:T(8,128)(2,1)} %param.7, s32[]{:T(128)S(6)} %select_n.4, bf16[512,704]{0,1:T(8,128)(2,1)} %param.6), kind=kLoop, calls=%fused_computation | loop fusion | bytes 1441796 | tf_op jit(solution)/shard_map/transpose | solution.py:331
  2.6 106.8 %block.1 = (bf16[256,2048]{1,0:T(8,128)(2,1)}, bf16[704,512]{1,0:T(8,128)(2,1)}, f32[8,704]{1,0:T(8,128)}) custom-call(bf16[352,512]{1,0:T(8,128)(2,1)} %get-tuple-element.10.gate, bf16[352,512]{1,0:T(8,128)(2,1)} %get-tuple-element.9.up, bf16[704,512]{1,0:T(8,128)(2,1)} %down.1, bf16[256,2048]{1,0:T(8,128)(2,1)} %tokens.1, bf16[256,2048]{1,0:T(8,128)(2,1)} %grad.1), custom_call_target="tpu_custom_call" | custom-call | tf_op jit(solution)/shard_map/block/pallas_call | solution.py:344
  109.4 3.0 %write.1 = (bf16[256,2048]{1,0:T(8,128)(2,1)}, f32[704,512]{1,0:T(8,128)}, f32[704]{0:T(1024)}) custom-call(bf16[256,2048]{1,0:T(8,128)(2,1)} %get-tuple-element.6.flow, bf16[704,512]{1,0:T(8,128)(2,1)} %get-tuple-element.7.shard, f32[8,704]{1,0:T(8,128)} %get-tuple-element.8.rows), custom_call_target="tpu_custom_call" | custom-call | tf_op jit(solution)/shard_map/write/pallas_call | solution.py:361
